TPU v7x, 32 devices: a whole 2x2x4 slice. The times are simulated.
32 devices in a mesh: grp: 2 (over y), fs: 4 (over z), tp: 4 (over x, core).
Axes of the slice: x: 2, y: 2, z: 4, core: 2. Of those that a mesh axis runs over, the one named last changes fastest.
Arguments:
- tokens: bfloat16 [1024, 2048], P(('grp', 'fs')), parts along dimension 0, may hold values from -12 to 12, as said below
- mix_heads: bfloat16 [1024, 2048], P(('grp', 'fs'), 'tp'), parts along dimension 0, may hold values from -6 to 6
- norm_first: float32 [2048], replicated, may hold values from 0.1 to 1.9
- gate_first: bfloat16 [2048, 5632], P('fs', 'tp'), may hold values from -0.125 to 0.125
- up_first: bfloat16 [2048, 5632], P('fs', 'tp'), may hold values from -0.125 to 0.125
- down_first: bfloat16 [5632, 2048], P('tp', 'fs'), may hold values from -0.078125 to 0.078125
- out_weight: bfloat16 [2048, 2048], P('tp', 'fs'), may hold values from -0.125 to 0.125
- norm_second: float32 [2048], replicated, may hold values from 0.1 to 1.9
- gate_second: bfloat16 [2048, 5632], P('fs', 'tp'), may hold values from -0.125 to 0.125
- up_second: bfloat16 [2048, 5632], P('fs', 'tp'), may hold values from -0.125 to 0.125
- down_second: bfloat16 [5632, 2048], P('tp', 'fs'), may hold values from -0.078125 to 0.078125
Outputs:
- layer_out: bfloat16 [1024, 2048], P(('grp', 'fs')), parts along dimension 0
There are 2 independent parts, one for each index of `grp`. A program takes and returns all parts, laid end to end along the dimension named above; an argument that names none is the same for every part. Nothing has to cross between parts.
Inputs may be any that keep to these rules, and one draw needn't show every extreme that they name: Each row of tokens carries a scale of its own.
All inputs are finite; a program needn't handle non-finite values.
Results may differ from a plain program's by a relative error of at most 0.014.
Values may be sent and summed in bfloat16 or wider, within the bound.
A program may use at most 64 MiB of HBM per device.

v0:
```python
import jax
import jax.numpy as jnp
from jax import lax
from jax.sharding import PartitionSpec as P

EPS = 0.1


def norm_rows(row_block, gain_vector):
    widened = row_block.astype(jnp.float32)
    scaled = widened * lax.rsqrt(jnp.mean(widened * widened, axis=-1, keepdims=True) + EPS)
    return (scaled * gain_vector).astype(jnp.bfloat16)


def gate_values(normed, gate_weight, value_weight):
    whole_gate, whole_values = (
        lax.all_gather(gate_weight, "fs", axis=0, tiled=True),
        lax.all_gather(value_weight, "fs", axis=0, tiled=True),
    )
    return (
        jnp.dot(normed, whole_gate, preferred_element_type=jnp.float32),
        jnp.dot(normed, whole_values, preferred_element_type=jnp.float32),
    )


def half_branch(normed, gate_weight, value_weight, down_weight):
    gates, values = gate_values(normed, gate_weight, value_weight)
    hidden = (jax.nn.silu(gates) * values).astype(jnp.bfloat16)
    return 0.5 * jnp.dot(
        hidden,
        lax.all_gather(down_weight, "fs", axis=1, tiled=True),
        preferred_element_type=jnp.float32,
    )


def share_sum(block_terms):
    return lax.psum_scatter(
        block_terms.astype(jnp.bfloat16), "tp", scatter_dimension=0, tiled=True
    ).astype(jnp.float32)


def join_rows(row_block):
    return lax.all_gather(row_block, "tp", axis=0, tiled=True)


def local(
    tokens,
    mix_heads,
    norm_first,
    gate_first,
    up_first,
    down_first,
    out_weight,
    norm_second,
    gate_second,
    up_second,
    down_second,
):
    normed_one = norm_rows(tokens, norm_first)
    first_terms = half_branch(normed_one, gate_first, up_first, down_first)
    heads_out = jnp.dot(
        mix_heads,
        lax.all_gather(out_weight, "fs", axis=1, tiled=True),
        preferred_element_type=jnp.float32,
    )
    first_terms = first_terms + heads_out
    share_rows = tokens.shape[0] // lax.axis_size("tp")
    offset = lax.axis_index("tp") * share_rows
    own_rows = lax.dynamic_slice_in_dim(tokens, offset, share_rows, 0).astype(jnp.float32)
    resid_two = own_rows + share_sum(first_terms)
    normed_two = join_rows(norm_rows(resid_two, norm_second))
    second_terms = half_branch(normed_two, gate_second, up_second, down_second)
    finished = (resid_two + share_sum(second_terms)).astype(jnp.bfloat16)
    return join_rows(finished)


def solution(mesh):
    in_specs = (
        P(("grp", "fs"), None),
        P(("grp", "fs"), "tp"),
        P(),
        P("fs", "tp"),
        P("fs", "tp"),
        P("tp", "fs"),
        P("tp", "fs"),
        P(),
        P("fs", "tp"),
        P("fs", "tp"),
        P("tp", "fs"),
    )
    out_specs = P(("grp", "fs"), None)
    return jax.shard_map(local, mesh=mesh, in_specs=in_specs, out_specs=out_specs, check_vma=False)
```

profile of v0, /device:TPU:0, one launch (start us, length us, event | category | flops | bytes accessed | tf_op | source)
XLA Modules:
  0.0 763.6 jit_solution(13067139635178607233)
XLA Ops:
  6.5 0.0 copy-start
  6.5 0.0 all-gather.8.cloned.1.call-start
  6.5 0.7 all-gather.8.cloned.1.call-update
  7.3 0.0 copy-start.1
  7.3 0.0 copy-start.3
  7.3 0.0 all-gather.10.cloned.1.call-start
  7.3 0.7 all-gather.10.cloned.1.call-update
  8.0 0.0 all-gather.12.cloned.1.call-start
  8.1 0.7 all-gather.12.cloned.1.call-update
  8.8 0.0 all-gather.14.cloned.1.call-start
  8.8 0.5 all-gather.14.cloned.1.call-update
  9.3 0.0 reduce-scatter.3.cloned.1.call-start
  9.4 1.2 fusion.4
  10.6 107.7 %all-gather.8.cloned.1.call-done = bf16[2048,1408]{1,0:T(8,128)(2,1)} async-done(((bf16[512,1408]{1,0:T(8,128)(2,1)}), bf16[2048,1408]{1,0:T(8,128)(2,1)}) %all-gather.8.cloned.1.call-update) | async-done | bytes 5767184 | tf_op jit(solution)/shard_map/all_gather | solution.py:17
  118.3 3.9 fusion.11
  122.2 102.7 %all-gather.10.cloned.1.call-done = bf16[2048,1408]{1,0:T(8,128)(2,1)} async-done(((bf16[512,1408]{1,0:T(8,128)(2,1)}), bf16[2048,1408]{1,0:T(8,128)(2,1)}) %all-gather.10.cloned.1.call-update) | async-done | bytes 5767184 | tf_op jit(solution)/shard_map/all_gather | solution.py:18
  224.9 106.5 %all-gather.12.cloned.1.call-done = bf16[1408,2048]{1,0:T(8,128)(2,1)} async-done(((bf16[1408,512]{1,0:T(8,128)(2,1)}), bf16[1408,2048]{1,0:T(8,128)(2,1)}) %all-gather.12.cloned.1.call-update) | async-done | bytes 5767184 | tf_op jit(solution)/shard_map/all_gather | solution.py:31
  331.5 0.0 copy-done.1
  331.5 0.0 copy-done.3
  331.5 6.3 convolution_multiply_fusion.3
  337.8 0.0 copy-start.4
  337.8 39.1 %all-gather.14.cloned.1.call-done = bf16[512,2048]{1,0:T(8,128)(2,1)} async-done(((bf16[512,512]{1,0:T(8,128)(2,1)}), bf16[512,2048]{1,0:T(8,128)(2,1)}) %all-gather.14.cloned.1.call-update) | async-done | bytes 2097168 | tf_op jit(solution)/shard_map/all_gather | solution.py:63
  376.8 0.0 copy-done
  376.8 2.8 fusion
  379.7 0.0 reduce-scatter.3.cloned.1.call-update
  379.7 0.0 all-gather.16.cloned.1.call-start
  379.8 0.5 all-gather.16.cloned.1.call-update
  380.3 0.0 all-gather.18.cloned.1.call-start
  380.3 0.7 all-gather.18.cloned.1.call-update
  381.0 0.0 all-gather.20.cloned.1.call-start
  381.1 0.7 all-gather.20.cloned.1.call-update
  381.8 0.0 reduce-scatter.5.cloned.1.call-start
  381.8 18.5 %reduce-scatter.3.cloned.1.call-done = bf16[32,2048]{1,0:T(8,128)(2,1)} async-done(((bf16[128,2048]{1,0:T(8,128)(2,1)}), bf16[32,2048]{1,0:T(8,128)(2,1)}) %reduce-scatter.3.cloned.1.call-update) | async-done | bytes 131088 | tf_op jit(solution)/shard_map/reduce_scatter | solution.py:37
  400.3 1.1 multiply_reduce_fusion
  401.4 0.0 copy-done.4
  401.4 1.0 multiply_convert_fusion
  402.4 6.6 all_gather.31
  409.0 99.5 %all-gather.16.cloned.1.call-done = bf16[2048,1408]{1,0:T(8,128)(2,1)} async-done(((bf16[512,1408]{1,0:T(8,128)(2,1)}), bf16[2048,1408]{1,0:T(8,128)(2,1)}) %all-gather.16.cloned.1.call-update) | async-done | bytes 5767184 | tf_op jit(solution)/shard_map/all_gather | solution.py:17
  508.5 3.6 fusion.15
  512.1 0.0 copy-start.2
  512.1 102.9 %all-gather.18.cloned.1.call-done = bf16[2048,1408]{1,0:T(8,128)(2,1)} async-done(((bf16[512,1408]{1,0:T(8,128)(2,1)}), bf16[2048,1408]{1,0:T(8,128)(2,1)}) %all-gather.18.cloned.1.call-update) | async-done | bytes 5767184 | tf_op jit(solution)/shard_map/all_gather | solution.py:18
  615.0 106.5 %all-gather.20.cloned.1.call-done = bf16[1408,2048]{1,0:T(8,128)(2,1)} async-done(((bf16[1408,512]{1,0:T(8,128)(2,1)}), bf16[1408,2048]{1,0:T(8,128)(2,1)}) %all-gather.20.cloned.1.call-update) | async-done | bytes 5767184 | tf_op jit(solution)/shard_map/all_gather | solution.py:31
  721.6 7.1 fusion.1
  728.6 0.0 reduce-scatter.5.cloned.1.call-update
  728.6 20.0 %reduce-scatter.5.cloned.1.call-done = bf16[32,2048]{1,0:T(8,128)(2,1)} async-done(((bf16[128,2048]{1,0:T(8,128)(2,1)}), bf16[32,2048]{1,0:T(8,128)(2,1)}) %reduce-scatter.5.cloned.1.call-update) | async-done | bytes 131088 | tf_op jit(solution)/shard_map/reduce_scatter | solution.py:37
  748.7 0.0 copy-done.2
  748.7 1.0 add_convert_fusion
  749.7 6.6 all_gather.35
  756.3 0.8 copy.13
  (2 shorter events, 0.0 us)
Async XLA Ops:
  6.5 370.3 %copy-start = (bf16[128,512]{1,0:T(8,128)(2,1)S(1)}, bf16[128,512]{1,0:T(8,128)(2,1)}, u32[]{:S(2)}) copy-start(bf16[128,512]{1,0:T(8,128)(2,1)} %param.12) | copy-start | bytes 393220
  6.5 111.8 %all-gather.8.cloned.1.call-start = ((), (), s32[]{:S(2)}) async-start(), calls=%async_computation.2 | async-start | bytes 7208960 | tf_op jit(solution)/shard_map/all_gather | solution.py:17
  7.3 324.2 %copy-start.1 = (bf16[128,2048]{1,0:T(8,128)(2,1)S(1)}, bf16[128,2048]{1,0:T(8,128)(2,1)}, u32[]{:S(2)}) copy-start(bf16[128,2048]{1,0:T(8,128)(2,1)} %param.11) | copy-start | bytes 1572868
  7.3 324.2 %copy-start.3 = (f32[2048]{0:T(1024)S(1)}, f32[2048]{0:T(1024)}, u32[]{:S(2)}) copy-start(f32[2048]{0:T(1024)} %param.13) | copy-start | bytes 24580
  7.3 217.6 %all-gather.10.cloned.1.call-start = ((), (), s32[]{:S(2)}) async-start(), calls=%async_computation.3 | async-start | bytes 7208960 | tf_op jit(solution)/shard_map/all_gather | solution.py:18
  8.0 323.4 %all-gather.12.cloned.1.call-start = ((), (), s32[]{:S(2)}) async-start(), calls=%async_computation.4 | async-start | bytes 7208960 | tf_op jit(solution)/shard_map/all_gather | solution.py:31
  8.8 368.1 %all-gather.14.cloned.1.call-start = ((), (), s32[]{:S(2)}) async-start(), calls=%async_computation.5 | async-start | bytes 2621440 | tf_op jit(solution)/shard_map/all_gather | solution.py:63
  9.3 391.0 %reduce-scatter.3.cloned.1.call-start = ((), (), s32[]{:S(2)}) async-start(), calls=%async_computation.6 | async-start | bytes 655360 | tf_op jit(solution)/shard_map/reduce_scatter | solution.py:37
  337.8 63.6 %copy-start.4 = (f32[2048]{0:T(1024)S(1)}, f32[2048]{0:T(1024)}, u32[]{:S(2)}) copy-start(f32[2048]{0:T(1024)} %param.18) | copy-start | bytes 24580
  379.7 128.8 %all-gather.16.cloned.1.call-start = ((), (), s32[]{:S(2)}) async-start(), calls=%async_computation.7 | async-start | bytes 7208960 | tf_op jit(solution)/shard_map/all_gather | solution.py:17
  380.3 234.7 %all-gather.18.cloned.1.call-start = ((), (), s32[]{:S(2)}) async-start(), calls=%async_computation.8 | async-start | bytes 7208960 | tf_op jit(solution)/shard_map/all_gather | solution.py:18
  381.0 340.5 %all-gather.20.cloned.1.call-start = ((), (), s32[]{:S(2)}) async-start(), calls=%async_computation.9 | async-start | bytes 7208960 | tf_op jit(solution)/shard_map/all_gather | solution.py:31
  381.8 366.9 %reduce-scatter.5.cloned.1.call-start = ((), (), s32[]{:S(2)}) async-start(), calls=%async_computation.10 | async-start | bytes 655360 | tf_op jit(solution)/shard_map/reduce_scatter | solution.py:37
  512.1 236.6 %copy-start.2 = (bf16[32,2048]{1,0:T(8,128)(2,1)S(1)}, bf16[32,2048]{1,0:T(8,128)(2,1)}, u32[]{:S(2)}) copy-start(bf16[32,2048]{1,0:T(8,128)(2,1)} %reduce-scatter.3.cloned.1.call-done) | copy-start | bytes 393220
Sparse Core Ops, SparseCore 0:
  8.9 109.3 all-gather.7
  119.9 104.9 all-gather.9
  226.5 104.9 all-gather.11
  332.9 43.9 all-gather.13
  379.8 20.4 reduce-scatter.2
  401.7 106.6 all-gather.15
  510.0 104.9 all-gather.17
  616.6 104.9 all-gather.19
  728.8 19.8 reduce-scatter.4
where the time goes:
time: 764 us
  waiting for transfers between devices  708 us (93%)
  matrix products  23.7 us (3%)
  between operations  13.3 us (2%)
  blocking collectives  13.2 us (2%)
    all_gather x2, waiting for transfers between devices, half_branch(): lax.all_gather(down_weight, 'fs', axis=1, tiled=True)  213 us
    all_gather x2, waiting for transfers between devices, gate_values(): lax.all_gather(gate_weight, 'fs', axis=0, tiled=True)  207 us
    all_gather x2, waiting for transfers between devices, gate_values(): lax.all_gather(value_weight, 'fs', axis=0, tiled=True)  206 us
    all_gather x1, waiting for transfers between devices, local(): lax.all_gather(out_weight, 'fs', axis=1, tiled=True)  39.1 us
    reduce_scatter x2, waiting for transfers between devices, share_sum(): lax.psum_scatter(block_terms.astype(jnp.bfloat16), 'tp', scatter_dimensio...  38.5 us
  transfers between devices with their start and end apart: 9, of which 9 were waited for; matrix products, arithmetic and copies ran while one was open for 2% of the time, Pallas kernels for 0%

commit v1 on v0

--- a/solution.py
+++ b/solution.py
@@ -4,6 +4,33 @@
 from jax.sharding import PartitionSpec as P
 
 EPS = 0.1
+
+
+def create_the_cubes(sample, net_axis):
+    raw_out = lax.axis_index(net_axis)
+    high = lax.axis_size(net_axis)
+    entries = []
+    val, current_arr, then = (high, raw_out, sample.shape[1])
+    for b in range(val):
+        entries.append((b, (b + 1) % val))
+    made = []
+    for b in range(val):
+        made.append((b, (b - 1) % val))
+    now = jnp.zeros((*sample.shape[:1], val * then, *sample.shape[2:]), sample.dtype)
+    now = lax.dynamic_update_slice_in_dim(now, sample, current_arr * then, axis=1)
+    work_now = clean = sample
+    found_now = val // 2
+    for src_i in range(1, found_now + 1):
+        work_now = lax.ppermute(work_now, net_axis, entries)
+        now = lax.dynamic_update_slice_in_dim(
+            now, work_now, (current_arr - src_i) % val * then, axis=1
+        )
+        if src_i < val - found_now:
+            clean = lax.ppermute(clean, net_axis, made)
+            now = lax.dynamic_update_slice_in_dim(
+                now, clean, (current_arr + src_i) % val * then, axis=1
+            )
+    return now
 
 
 def norm_rows(row_block, gain_vector):
@@ -27,9 +54,7 @@
     gates, values = gate_values(normed, gate_weight, value_weight)
     hidden = (jax.nn.silu(gates) * values).astype(jnp.bfloat16)
     return 0.5 * jnp.dot(
-        hidden,
-        lax.all_gather(down_weight, "fs", axis=1, tiled=True),
-        preferred_element_type=jnp.float32,
+        hidden, create_the_cubes(down_weight, "fs"), preferred_element_type=jnp.float32
     )
 
 

time: 764 us -> 690 us (0.903)
  waiting for transfers between devices: 708 us -> 575 us
  starting transfers between devices: 0.31 us -> 35.8 us
  local copies, waits for them, and re-layouts: 0.82 us -> 22.6 us
    ppermute x0 -> x6, waiting for transfers between devices: none -> 273 us  [the longest x4 158 us: create_the_cubes(): work_now = lax.ppermute(work_now, net_axis, entries)]
    all_gather x2 -> x0, waiting for transfers between devices: 213 us -> none  [half_branch(): lax.all_gather(down_weight, 'fs', axis=1, tiled=True)]
    all_gather x2, waiting for transfers between devices: 207 us -> 70.9 us  [gate_values(): lax.all_gather(gate_weight, 'fs', axis=0, tiled=True)]
    all_gather x1, waiting for transfers between devices: 39.1 us -> 0.01 us  [local(): lax.all_gather(out_weight, 'fs', axis=1, tiled=True)]
    ppermute x0 -> x6, starting transfers between devices: none -> 35.6 us  [the longest x4 29.7 us: create_the_cubes(): work_now = lax.ppermute(work_now, net_axis, entries)]
    reduce_scatter x2, waiting for transfers between devices: 38.5 us -> 20 us  [share_sum(): lax.psum_scatter(block_terms.astype(jnp.bfloat16), 'tp', scatter_dimensio...]
    dynamic_update_slice x0 -> x8, local copies, waits for them, and re-layouts: none -> 15.4 us  [the longest x4 7.71 us: create_the_cubes(): lax.dynamic_update_slice_in_dim(now, work_now, (current_arr - src_i) % va...]
  transfers between devices with their start and end apart: 9 -> 13, of which waited for: 9 -> 11; matrix products, arithmetic and copies ran while one was open for 2% -> 5% of each run, Pallas kernels for 0% -> 0%
where the time goes in v1:
time: 690 us; the launch traced here: 689 us
  waiting for transfers between devices  575 us (83%)
  starting transfers between devices  35.8 us (5%)
  matrix products  24.5 us (4%)
  local copies, waits for them, and re-layouts  22.6 us (3%)
  blocking collectives  13.8 us (2%)
  between operations  13.6 us (2%)
    all_gather x2, waiting for transfers between devices, gate_values(): lax.all_gather(value_weight, 'fs', axis=0, tiled=True)  207 us
    ppermute x4, waiting for transfers between devices, create_the_cubes(): work_now = lax.ppermute(work_now, net_axis, entries)  158 us
    ppermute x2, waiting for transfers between devices, create_the_cubes(): clean = lax.ppermute(clean, net_axis, made)  116 us
    all_gather x2, waiting for transfers between devices, gate_values(): lax.all_gather(gate_weight, 'fs', axis=0, tiled=True)  70.9 us
    ppermute x4, starting transfers between devices, create_the_cubes(): work_now = lax.ppermute(work_now, net_axis, entries)  29.7 us
    reduce_scatter x2, waiting for transfers between devices, share_sum(): lax.psum_scatter(block_terms.astype(jnp.bfloat16), 'tp', scatter_dimensio...  20 us
    dot_general x2, matrix products, half_branch(): jnp.dot(hidden, create_the_cubes(down_weight, 'fs'), preferred_element_ty...  14.3 us
  transfers between devices with their start and end apart: 13, of which 11 were waited for; matrix products, arithmetic and copies ran while one was open for 5% of the time, Pallas kernels for 0%

profile of v1, /device:TPU:0, one launch (start us, length us, event | category | flops | bytes accessed | tf_op | source)
XLA Modules:
  0.0 689.4 jit_solution(4010602772304346363)
XLA Ops:
  6.5 0.0 copy-start
  6.5 0.0 copy-start.2
  6.5 0.0 all-gather.10.cloned.1.call-start
  6.5 0.7 all-gather.10.cloned.1.call-update
  7.3 0.0 all-gather.6.cloned.1.call-start
  7.3 0.7 all-gather.6.cloned.1.call-update
  8.0 0.0 all-gather.8.cloned.1.call-start
  8.1 0.7 all-gather.8.cloned.1.call-update
  8.7 0.0 reduce-scatter.3.cloned.1.call-start
  8.8 3.1 collective-permute-start
  11.9 2.1 collective-permute-start.1
  14.0 55.3 %collective-permute-done = bf16[1408,512]{1,0:T(8,128)(2,1)S(1)} collective-permute-done((bf16[1408,512]{1,0:T(8,128)(2,1)}, bf16[1408,512]{1,0:T(8,128)(2,1)S(1)}, u32[]{:S(2)}, u32[]{:S(2)}) %collective-permute-start) | collective-permute-done | bytes 1441824 | tf_op jit(solution)/shard_map/ppermute | solution.py:24
  69.3 26.5 %collective-permute-start.2 = (bf16[1408,512]{1,0:T(8,128)(2,1)S(1)}, bf16[1408,512]{1,0:T(8,128)(2,1)}, u32[]{:S(2)}, u32[]{:S(2)}) collective-permute-start(bf16[1408,512]{1,0:T(8,128)(2,1)S(1)} %collective-permute-done), channel_id=1, source_target_pairs={{0,4},{4,8},{8,12},{12,0},{1,5},{5,9},{9,13},{13,1},{2,6},{6,10},{... | collective-permute-start | bytes 4325384 | tf_op jit(solution)/shard_map/ppermute | solution.py:24
  95.8 1.2 fusion.5
  97.1 3.2 broadcast.36.clone.1
  100.3 0.0 copy-done.2
  100.3 1.2 constant_dynamic-update-slice_fusion.7
  101.5 0.0 copy-start.1
  101.5 1.2 constant_dynamic-update-slice_fusion.6
  102.8 11.4 %collective-permute-done.1 = bf16[1408,512]{1,0:T(8,128)(2,1)} collective-permute-done((bf16[1408,512]{1,0:T(8,128)(2,1)}, bf16[1408,512]{1,0:T(8,128)(2,1)}, u32[]{:S(2)}, u32[]{:S(2)}) %collective-permute-start.1) | collective-permute-done | bytes 1441824 | tf_op jit(solution)/shard_map/ppermute | solution.py:29
  114.2 2.6 constant_dynamic-update-slice_fusion.5
  116.8 57.2 %collective-permute-done.2 = bf16[1408,512]{1,0:T(8,128)(2,1)} collective-permute-done((bf16[1408,512]{1,0:T(8,128)(2,1)S(1)}, bf16[1408,512]{1,0:T(8,128)(2,1)}, u32[]{:S(2)}, u32[]{:S(2)}) %collective-permute-start.2) | collective-permute-done | bytes 1441824 | tf_op jit(solution)/shard_map/ppermute | solution.py:24
  174.0 2.6 constant_dynamic-update-slice_fusion.4
  176.6 0.0 copy-done
  176.6 2.1 fusion.16
  178.7 55.9 %all-gather.6.cloned.1.call-done = bf16[2048,1408]{1,0:T(8,128)(2,1)} async-done(((bf16[512,1408]{1,0:T(8,128)(2,1)}), bf16[2048,1408]{1,0:T(8,128)(2,1)}) %all-gather.6.cloned.1.call-update) | async-done | bytes 5767184 | tf_op jit(solution)/shard_map/all_gather | solution.py:44
  234.6 0.0 copy-done.1
  234.6 0.0 copy-done.5
  234.6 4.5 fusion.12
  239.1 102.8 %all-gather.8.cloned.1.call-done = bf16[2048,1408]{1,0:T(8,128)(2,1)} async-done(((bf16[512,1408]{1,0:T(8,128)(2,1)}), bf16[2048,1408]{1,0:T(8,128)(2,1)}) %all-gather.8.cloned.1.call-update) | async-done | bytes 5767184 | tf_op jit(solution)/shard_map/all_gather | solution.py:45
  341.9 7.3 %fusion.1 = bf16[128,2048]{1,0:T(8,128)(2,1)} fusion(f32[128,2048]{1,0:T(8,128)S(1)} %fusion.16, bf16[1408,2048]{1,0:T(8,128)(2,1)} %constant_dynamic-update-slice_fusion.4, bf16[2048,1408]{1,0:T(8,128)(2,1)} %all-gather.8.cloned.1.call-done, f32[128,1408]{1,0:T(8,128)} %fusion.12, bf16[128,2048]{1,0:T(8,128)(2,1)S(1)} %copy-done.1, f32[2048]{0:T(1024)S(1)} %copy-done.5, ...), kind=kOutput, calls=%fused_computation.5 | convolution fusion | flops 1479311360 | bytes 14361088 | tf_op jit(solution)/shard_map/dot_general | solution.py:56
  349.2 0.0 reduce-scatter.3.cloned.1.call-update
  349.2 0.0 all-gather.12.cloned.1.call-start
  349.3 0.5 all-gather.12.cloned.1.call-update
  349.8 0.0 all-gather.14.cloned.1.call-start
  349.9 0.5 all-gather.14.cloned.1.call-update
  350.4 0.0 reduce-scatter.5.cloned.1.call-start
  350.4 0.0 copy-done.3
  350.5 0.1 collective-permute-start.3
  350.5 3.8 collective-permute-start.4
  354.3 35.2 %collective-permute-done.3 = bf16[1408,512]{1,0:T(8,128)(2,1)S(1)} collective-permute-done((bf16[1408,512]{1,0:T(8,128)(2,1)S(1)}, bf16[1408,512]{1,0:T(8,128)(2,1)S(1)}, u32[]{:S(2)}, u32[]{:S(2)}) %collective-permute-start.3) | collective-permute-done | bytes 1441824 | tf_op jit(solution)/shard_map/ppermute | solution.py:24
  389.5 0.0 collective-permute-start.5
  389.5 3.2 broadcast.36.clone
  392.7 1.2 constant_dynamic-update-slice_fusion.3
  393.9 1.2 constant_dynamic-update-slice_fusion.2
  395.2 104.4 %collective-permute-done.4 = bf16[1408,512]{1,0:T(8,128)(2,1)} collective-permute-done((bf16[1408,512]{1,0:T(8,128)(2,1)S(1)}, bf16[1408,512]{1,0:T(8,128)(2,1)}, u32[]{:S(2)}, u32[]{:S(2)}) %collective-permute-start.4) | collective-permute-done | bytes 1441824 | tf_op jit(solution)/shard_map/ppermute | solution.py:29
  499.6 2.6 constant_dynamic-update-slice_fusion.1
  502.2 10.0 %collective-permute-done.5 = bf16[1408,512]{1,0:T(8,128)(2,1)} collective-permute-done((bf16[1408,512]{1,0:T(8,128)(2,1)S(1)}, bf16[1408,512]{1,0:T(8,128)(2,1)}, u32[]{:S(2)}, u32[]{:S(2)}) %collective-permute-start.5) | collective-permute-done | bytes 1441824 | tf_op jit(solution)/shard_map/ppermute | solution.py:24
  512.2 2.6 constant_dynamic-update-slice_fusion
  514.8 1.1 multiply_reduce_fusion
  515.9 0.0 copy-done.6
  515.9 1.0 multiply_convert_fusion
  516.9 7.1 %all_gather.24 = bf16[128,2048]{1,0:T(8,128)(2,1)S(1)} all-gather(bf16[32,2048]{1,0:T(8,128)(2,1)S(1)} %multiply_convert_fusion), channel_id=1, replica_groups=mesh['grp'=2,'fs'=4,'tp'=4] {'tp'}, dimensions={0}, use_global_device_ids=true | all-gather | bytes 655360 | tf_op jit(solution)/shard_map/all_gather | solution.py:68
  524.0 15.0 %all-gather.12.cloned.1.call-done = bf16[2048,1408]{1,0:T(8,128)(2,1)} async-done(((bf16[512,1408]{1,0:T(8,128)(2,1)}), bf16[2048,1408]{1,0:T(8,128)(2,1)}) %all-gather.12.cloned.1.call-update) | async-done | bytes 5767184 | tf_op jit(solution)/shard_map/all_gather | solution.py:44
  539.0 3.6 fusion.17
  542.7 0.0 copy-start.4
  542.7 104.4 %all-gather.14.cloned.1.call-done = bf16[2048,1408]{1,0:T(8,128)(2,1)} async-done(((bf16[512,1408]{1,0:T(8,128)(2,1)}), bf16[2048,1408]{1,0:T(8,128)(2,1)}) %all-gather.14.cloned.1.call-update) | async-done | bytes 5767184 | tf_op jit(solution)/shard_map/all_gather | solution.py:45
  647.0 7.1 %fusion.2 = bf16[128,2048]{1,0:T(8,128)(2,1)} fusion(bf16[1408,2048]{1,0:T(8,128)(2,1)} %constant_dynamic-update-slice_fusion, bf16[128,2048]{1,0:T(8,128)(2,1)S(1)} %all_gather.24, bf16[2048,1408]{1,0:T(8,128)(2,1)} %all-gather.14.cloned.1.call-done, f32[128,1408]{1,0:T(8,128)S(1)} %fusion.17), kind=kOutput, calls=%fused_computation.6 | convolution fusion | flops 1478000640 | bytes 13303808 | tf_op jit(solution)/shard_map/dot_general | solution.py:56
  654.1 0.0 reduce-scatter.5.cloned.1.call-update
  654.1 20.0 %reduce-scatter.5.cloned.1.call-done = bf16[32,2048]{1,0:T(8,128)(2,1)} async-done(((bf16[128,2048]{1,0:T(8,128)(2,1)}), bf16[32,2048]{1,0:T(8,128)(2,1)}) %reduce-scatter.5.cloned.1.call-update) | async-done | bytes 131088 | tf_op jit(solution)/shard_map/reduce_scatter | solution.py:62
  674.1 0.0 copy-done.4
  674.2 1.0 add_convert_fusion
  675.1 6.6 all_gather.27
  681.7 0.8 copy.21
  (7 shorter events, 0.0 us)
Async XLA Ops:
  6.5 170.1 %copy-start = (bf16[128,512]{1,0:T(8,128)(2,1)S(1)}, bf16[128,512]{1,0:T(8,128)(2,1)}, u32[]{:S(2)}) copy-start(bf16[128,512]{1,0:T(8,128)(2,1)} %param.12) | copy-start | bytes 393220
  6.5 93.7 %copy-start.2 = (bf16[1408,512]{1,0:T(8,128)(2,1)S(1)}, bf16[1408,512]{1,0:T(8,128)(2,1)}, u32[]{:S(2)}) copy-start(bf16[1408,512]{1,0:T(8,128)(2,1)} %param.16) | copy-start | bytes 4325380
  6.5 170.1 %all-gather.10.cloned.1.call-start = ((), (), s32[]{:S(2)}) async-start(), calls=%async_computation.4 | async-start | bytes 2621440 | tf_op jit(solution)/shard_map/all_gather | solution.py:88
  7.3 227.3 %all-gather.6.cloned.1.call-start = ((), (), s32[]{:S(2)}) async-start(), calls=%async_computation.2 | async-start | bytes 7208960 | tf_op jit(solution)/shard_map/all_gather | solution.py:44
  8.0 333.9 %all-gather.8.cloned.1.call-start = ((), (), s32[]{:S(2)}) async-start(), calls=%async_computation.3 | async-start | bytes 7208960 | tf_op jit(solution)/shard_map/all_gather | solution.py:45
  8.7 506.1 %reduce-scatter.3.cloned.1.call-start = ((), (), s32[]{:S(2)}) async-start(), calls=%async_computation.5 | async-start | bytes 655360 | tf_op jit(solution)/shard_map/reduce_scatter | solution.py:62
  8.8 60.5 %collective-permute-start = (bf16[1408,512]{1,0:T(8,128)(2,1)}, bf16[1408,512]{1,0:T(8,128)(2,1)S(1)}, u32[]{:S(2)}, u32[]{:S(2)}) collective-permute-start(bf16[1408,512]{1,0:T(8,128)(2,1)} %param.16), channel_id=1, source_target_pairs={{0,4},{4,8},{8,12},{12,0},{1,5},{5,9},{9,13},{13,1},{2,6},{6,10},{... | collective-permute-start | bytes 4325384 | tf_op jit(solution)/shard_map/ppermute | solution.py:24
  11.9 102.3 %collective-permute-start.1 = (bf16[1408,512]{1,0:T(8,128)(2,1)}, bf16[1408,512]{1,0:T(8,128)(2,1)}, u32[]{:S(2)}, u32[]{:S(2)}) collective-permute-start(bf16[1408,512]{1,0:T(8,128)(2,1)} %param.16), channel_id=1, source_target_pairs={{0,12},{4,0},{8,4},{12,8},{1,13},{5,1},{9,5},{13,9},{2,14},{6,2},{... | collective-permute-start | bytes 4325384 | tf_op jit(solution)/shard_map/ppermute | solution.py:29
  69.3 104.7 %collective-permute-start.2 = (bf16[1408,512]{1,0:T(8,128)(2,1)S(1)}, bf16[1408,512]{1,0:T(8,128)(2,1)}, u32[]{:S(2)}, u32[]{:S(2)}) collective-permute-start(bf16[1408,512]{1,0:T(8,128)(2,1)S(1)} %collective-permute-done), channel_id=1, source_target_pairs={{0,4},{4,8},{8,12},{12,0},{1,5},{5,9},{9,13},{13,1},{2,6},{6,10},{... | collective-permute-start | bytes 4325384 | tf_op jit(solution)/shard_map/ppermute | solution.py:24
  101.5 133.1 %copy-start.1 = (bf16[128,2048]{1,0:T(8,128)(2,1)S(1)}, bf16[128,2048]{1,0:T(8,128)(2,1)}, u32[]{:S(2)}) copy-start(bf16[128,2048]{1,0:T(8,128)(2,1)} %param.11) | copy-start | bytes 1572868
  101.5 133.1 %copy-start.5 = (f32[2048]{0:T(1024)S(1)}, f32[2048]{0:T(1024)}, u32[]{:S(2)}) copy-start(f32[2048]{0:T(1024)} %param.13) | copy-start | bytes 24580
  239.1 111.3 %copy-start.3 = (bf16[1408,512]{1,0:T(8,128)(2,1)S(1)}, bf16[1408,512]{1,0:T(8,128)(2,1)}, u32[]{:S(2)}) copy-start(bf16[1408,512]{1,0:T(8,128)(2,1)} %param.21) | copy-start | bytes 4325380
  349.2 189.8 %all-gather.12.cloned.1.call-start = ((), (), s32[]{:S(2)}) async-start(), calls=%async_computation.6 | async-start | bytes 7208960 | tf_op jit(solution)/shard_map/all_gather | solution.py:44
  349.8 297.2 %all-gather.14.cloned.1.call-start = ((), (), s32[]{:S(2)}) async-start(), calls=%async_computation.7 | async-start | bytes 7208960 | tf_op jit(solution)/shard_map/all_gather | solution.py:45
  350.4 323.7 %reduce-scatter.5.cloned.1.call-start = ((), (), s32[]{:S(2)}) async-start(), calls=%async_computation.8 | async-start | bytes 655360 | tf_op jit(solution)/shard_map/reduce_scatter | solution.py:62
  350.5 39.1 %collective-permute-start.3 = (bf16[1408,512]{1,0:T(8,128)(2,1)S(1)}, bf16[1408,512]{1,0:T(8,128)(2,1)S(1)}, u32[]{:S(2)}, u32[]{:S(2)}) collective-permute-start(bf16[1408,512]{1,0:T(8,128)(2,1)S(1)} %copy-done.3), channel_id=1, source_target_pairs={{0,4},{4,8},{8,12},{12,0},{1,5},{5,9},{9,13},{13,1},{2,6},{6,10},{... | collective-permute-start | bytes 4325384 | tf_op jit(solution)/shard_map/ppermute | solution.py:24
  350.5 149.0 %collective-permute-start.4 = (bf16[1408,512]{1,0:T(8,128)(2,1)S(1)}, bf16[1408,512]{1,0:T(8,128)(2,1)}, u32[]{:S(2)}, u32[]{:S(2)}) collective-permute-start(bf16[1408,512]{1,0:T(8,128)(2,1)S(1)} %copy-done.3), channel_id=1, source_target_pairs={{0,12},{4,0},{8,4},{12,8},{1,13},{5,1},{9,5},{13,9},{2,14},{6,2},{... | collective-permute-start | bytes 4325384 | tf_op jit(solution)/shard_map/ppermute | solution.py:29
  389.5 122.7 %collective-permute-start.5 = (bf16[1408,512]{1,0:T(8,128)(2,1)S(1)}, bf16[1408,512]{1,0:T(8,128)(2,1)}, u32[]{:S(2)}, u32[]{:S(2)}) collective-permute-start(bf16[1408,512]{1,0:T(8,128)(2,1)S(1)} %collective-permute-done.3), channel_id=1, source_target_pairs={{0,4},{4,8},{8,12},{12,0},{1,5},{5,9},{9,13},{13,1},{2,6},{6,10},{... | collective-permute-start | bytes 4325384 | tf_op jit(solution)/shard_map/ppermute | solution.py:24
  392.7 123.2 %copy-start.6 = (f32[2048]{0:T(1024)S(1)}, f32[2048]{0:T(1024)}, u32[]{:S(2)}) copy-start(f32[2048]{0:T(1024)} %param.18) | copy-start | bytes 24580
  542.7 131.5 %copy-start.4 = (bf16[32,2048]{1,0:T(8,128)(2,1)S(1)}, bf16[32,2048]{1,0:T(8,128)(2,1)}, u32[]{:S(2)}) copy-start(bf16[32,2048]{1,0:T(8,128)(2,1)} %reduce-scatter.3.cloned.1.call-done) | copy-start | bytes 393220
Sparse Core Ops, SparseCore 0:
  8.9 87.7 all-gather.9
  98.3 136.2 all-gather.5
  236.1 105.7 all-gather.7
  349.4 19.8 reduce-scatter.2
  370.7 168.2 all-gather.11
  540.5 106.5 all-gather.13
  654.2 19.8 reduce-scatter.4
